TPU v7x, 512 devices: a whole 4x8x8 slice. The times are simulated.
512 devices in a mesh: sp: 256 (over z, y, x), tp: 2 (over core).
Axes of the slice: x: 4, y: 8, z: 8, core: 2. Of those that a mesh axis runs over, the one named last changes fastest.
Arguments:
- tokens: bfloat16 [32768, 2048], P('sp', 'tp'), may hold values from -6 to 6
- in_gain: bfloat16 [1, 2048], P(None, 'tp'), may hold values from 0.099609375 to 1.8984375
- w_input: bfloat16 [2048, 1024], P(None, 'tp'), may hold values from -0.125 to 0.125
- w_bgate: bfloat16 [2048, 1024], P(None, 'tp'), may hold values from -0.125 to 0.125
- w_cgate: bfloat16 [2048, 1024], P(None, 'tp'), may hold values from -0.125 to 0.125
- w_value: bfloat16 [2048, 1024], P(None, 'tp'), may hold values from -0.125 to 0.125
- decay_rate: float32 [64, 64], P('tp'), may hold values from 6.1035156e-06 to 0.034, as said below
- angle: float32 [64, 64], P('tp'), may hold values from -3.140625 to 3.140625
- decay_shift: float32 [64, 32768], P('tp', 'sp'), may hold values from -1.1 to 0, as said below
- b_input: float32 [2, 64, 64, 16], P(None, 'tp'), may hold values from -1 to 1
- c_output: float32 [2, 64, 16, 64], P(None, 'tp'), may hold values from -0.75 to 0.75
- initial_recurrence_vector: float32 [2, 64, 64], P(None, 'tp'), may hold values from -1086.116 to 1086.116
- skip_gain: float32 [1024], P('tp'), may hold values from -4 to 4
- ssm_gain: float32 [1024], P('tp'), may hold values from 0.1 to 1.9
- conv_gain: float32 [1024], P('tp'), may hold values from 0.1 to 1.9
- conv_taps: float32 [3, 1024], P(None, 'tp'), may hold values from -3.5 to 3.5
- w_out_ssm: bfloat16 [1024, 2048], P('tp'), may hold values from -0.125 to 0.125
- w_out_conv: bfloat16 [1024, 2048], P('tp'), may hold values from -0.125 to 0.125
Outputs:
- mixed: bfloat16 [32768, 2048], P(('sp', 'tp'))
Inputs may be any that keep to these rules, and one draw needn't show every extreme that they name: `decay_rate`: positive rates. `decay_shift`: never positive.
All inputs are finite; a program needn't handle non-finite values.
Results may differ from a plain program's by a relative error of at most 0.0085.
Values may be sent and summed in bfloat16 or wider, within the bound.
A program may use at most 64 MiB of HBM per device.

v0:
```python
import functools
import math

import jax
import jax.numpy as jnp
from jax import lax
from jax.experimental import pallas as pl
from jax.experimental.pallas import tpu as pltpu
from jax.sharding import Mesh
from jax.sharding import PartitionSpec as P

D = 2048
HALF = 1024
CH = 512
GROUPS = 32
ENTRIES = 64
ROWS = 128
PAIRS = 16
SP_DIMS = (8, 8, 4)
SP = ("sz", "sy", "sx")
F32 = jnp.float32
BF16 = jnp.bfloat16
HIGHEST = lax.Precision.HIGHEST


def cmul(a, b):
    return (a[0] * b[0] - a[1] * b[1], a[0] * b[1] + a[1] * b[0])


def cadd(a, b):
    return (a[0] + b[0], a[1] + b[1])


def expm1(v):
    series = 1.0 + v / 8.0
    for k in range(7, 1, -1):
        series = 1.0 + series * v / k
    return jnp.where(jnp.abs(v) < 0.3, v * series, jnp.exp(v) - 1.0)


def split(v):
    high = v.astype(BF16)
    return high, (v - high.astype(F32)).astype(BF16)


def iota(shape, dim):
    return lax.broadcasted_iota(jnp.int32, shape, dim)


def kernel(
    dims,
    tokens,
    in_gain,
    w_input,
    w_bgate,
    w_cgate,
    w_value,
    decay_rate,
    angle,
    decay_shift,
    b_input,
    c_output,
    initial,
    skip_gain,
    ssm_gain,
    conv_gain,
    conv_taps,
    w_out_ssm,
    w_out_conv,
    out,
    tok_v,
    gain_v,
    win_v,
    wb_v,
    wc_v,
    wv_v,
    rate_v,
    angle_v,
    shift_v,
    b_v,
    c_v,
    init_v,
    skip_v,
    sgain_v,
    cgain_v,
    taps_v,
    wos_v,
    woc_v,
    acc_v,
    u_v,
    bw_v,
    cw_v,
    ce_v,
    expf_v,
    at_v,
    bt_v,
    wneg_v,
    wpos_v,
    wposb_v,
    q_v,
    sum_v,
    mixed_v,
    ypre_v,
    pad_v,
    bg_v,
    cpart_v,
    sout_v,
    part_v,
    got_v,
    sx_v,
    sy_v,
    sz_v,
    mx_v,
    my_v,
    mz_v,
    load_sem,
    tok_sem,
    tail_sem,
    part_ss,
    part_rs,
    sx_sem,
    sy_sem,
    sz_sem,
    mx_sem,
    my_sem,
    mz_sem,
    ring2,
    ring3,
    zring2,
    zring3,
    zring4,
):
    nz, ny, nx = dims
    z, y, x = (lax.axis_index(a) for a in SP)
    tp = lax.axis_index("tp")
    other = 1 - tp
    coords = {"sz": (z, nz), "sy": (y, ny), "sx": (x, nx)}

    pairs = [
        (tokens, tok_v.at[tp]),
        (in_gain, gain_v.at[tp]),
        (w_input.at[pl.ds(tp * HALF, HALF)], win_v.at[pl.ds(tp * HALF, HALF)]),
        (decay_shift, shift_v),
        (decay_rate, rate_v),
        (angle, angle_v),
        (w_input.at[pl.ds(other * HALF, HALF)], win_v.at[pl.ds(other * HALF, HALF)]),
        (b_input, b_v),
        (w_cgate, wc_v),
        (w_value, wv_v),
        (c_output, c_v),
        (w_bgate, wb_v),
        (initial, init_v),
        (skip_gain, skip_v),
        (ssm_gain, sgain_v),
        (conv_gain, cgain_v),
        (conv_taps, taps_v),
        (w_out_conv, woc_v),
        (w_out_ssm, wos_v),
    ]
    loads = [pltpu.make_async_copy(s, d, load_sem.at[k]) for k, (s, d) in enumerate(pairs)]
    for k in (0, 1, 3, 4, 5, 2, 7, 6):
        loads[k].start()

    def near(axis):
        n = coords[axis][1]
        return [] if n == 1 else ([1] if n == 2 else [1, n - 1])

    def at_step(axis, step):
        here, n = coords[axis]
        return {axis: lax.rem(here + step, n)}

    around = [at_step(a, s) for a in ("sy", "sx") for s in near(a)]
    far = [at_step("sx", s) for s in near("sx")]
    far += [at_step("sy", s) for s in (2, 6) if ny == 8]

    def tell(sem, step, above=True):
        @pl.when(z >= step)
        def _():
            pl.semaphore_signal(sem, inc=1, device_id={"sz": z - step})

        if above:

            @pl.when(z + step < nz)
            def _():
                pl.semaphore_signal(sem, inc=1, device_id={"sz": z + step})

    def beside(step):
        return jnp.where(z + step < nz, 1, 0) + jnp.where(z >= step, 1, 0)

    barrier = pltpu.get_barrier_semaphore()
    for dev in [{"tp": other}] + around:
        pl.semaphore_signal(barrier, inc=1, device_id=dev)
    tell(barrier, 1)

    loads[0].wait()
    loads[1].wait()
    pl.semaphore_wait(barrier, 1 + len(around) + beside(1))

    tok_copy = pltpu.make_async_remote_copy(
        tok_v.at[tp], tok_v.at[tp], tok_sem.at[0], tok_sem.at[1], device_id={"tp": other}
    )
    gain_copy = pltpu.make_async_remote_copy(
        gain_v.at[tp], gain_v.at[tp], tok_sem.at[2], tok_sem.at[3], device_id={"tp": other}
    )
    tok_copy.start()
    gain_copy.start()
    for dev in around:
        pl.semaphore_signal(ring2, inc=1, device_id=dev)
    if nz > 2:
        tell(zring2, 1)
    for k in range(8, len(loads)):
        loads[k].start()

    def exchange(buf, sems, axis, later):
        here, n = coords[axis]
        order = sorted(range(1, n), key=lambda s: -min(s, n - s))

        def copy(step):
            return pltpu.make_async_remote_copy(
                buf.at[here],
                buf.at[here],
                sems.at[0, step],
                sems.at[1, step],
                device_id=at_step(axis, step),
            )

        def start():
            for s in order:
                if later:
                    pl.when(here + s < n)(copy(s).start)
                else:
                    copy(s).start()

        def incoming(step):
            slot = lax.rem(here + n - step, n)
            return pltpu.make_async_remote_copy(
                buf.at[slot],
                buf.at[slot],
                sems.at[0, step],
                sems.at[1, step],
                device_id=at_step(axis, step),
            )

        def wait_recv():
            for s in range(1, n):
                if later:
                    pl.when(here >= s)(incoming(s).wait_recv)
                else:
                    incoming(s).wait_recv()

        def wait_send():
            for s in range(1, n):
                if later:
                    pl.when(here + s < n)(copy(s).wait_send)
                else:
                    copy(s).wait_send()

        return start, wait_recv, wait_send

    sx = exchange(sx_v, sx_sem, "sx", False)
    sy = exchange(sy_v, sy_sem, "sy", False)
    sz = exchange(sz_v, sz_sem, "sz", True)
    mx = exchange(mx_v, mx_sem, "sx", False)
    my = exchange(my_v, my_sem, "sy", False)
    mz = exchange(mz_v, mz_sem, "sz", True)

    def half(which):
        floats = tok_v[which].astype(F32)
        scaled = (floats * gain_v[which].astype(F32)).astype(BF16)
        return scaled, jnp.sum(floats * floats, axis=1, keepdims=True)

    loads[3].wait()
    tri = (iota((ROWS, ROWS), 0) >= iota((ROWS, ROWS), 1)).astype(F32)
    shifts = jnp.concatenate([shift_v[...], jnp.zeros((ROWS - GROUPS, ROWS), F32)], axis=0)
    logs = lax.dot_general(
        tri, shifts, (((1,), (1,)), ((), ())), precision=HIGHEST, preferred_element_type=F32
    )
    sigma = logs[ROWS - 1 : ROWS]
    mid = logs[ROWS // 2 - 1 : ROWS // 2]
    sx_v[x] = sigma

    loads[4].wait()
    loads[5].wait()

    def paired(ref, lead=()):
        even = ref[(*lead, pl.ds(0, PAIRS, 2), slice(None))]
        odd = ref[(*lead, pl.ds(1, PAIRS, 2), slice(None))]
        return jnp.concatenate([even, odd], axis=1)

    rate = paired(rate_v)
    theta = paired(angle_v)

    def power(k):
        mag = jnp.exp(-rate * float(k))
        ph = theta * float(k)
        return (mag * jnp.cos(ph), mag * jnp.sin(ph))

    cos1, sin1 = jnp.cos(theta), jnp.sin(theta)
    unit = (cos1, sin1)
    lane = iota((1, ROWS), 1)
    grp = iota((PAIRS, ROWS), 0)
    grp_lane = iota((PAIRS, ROWS), 1)
    spread_h = (
        (iota((ROWS, ROWS), 0) % 2 == iota((ROWS, ROWS), 1) // ENTRIES)
        & (iota((ROWS, ROWS), 0) < GROUPS)
    ).astype(F32)

    def expand(rows):
        blocks = [jnp.where(grp_lane // 2 == grp, row, 0.0) for row in rows]
        wide = jnp.dot(
            jnp.concatenate(blocks, axis=0), spread_h, precision=HIGHEST, preferred_element_type=F32
        )
        return [wide[PAIRS * k : PAIRS * (k + 1)] for k in range(len(rows))]

    keep = lane < GROUPS
    ratio = jnp.concatenate([jnp.exp(mid - logs), jnp.exp(logs - mid)], axis=0)
    ratio = jnp.where(keep, ratio, 0.0)
    hi = ratio.astype(BF16)
    lo = ratio - hi.astype(F32)
    both = hi.astype(F32) + pltpu.roll(lo, GROUPS, 1)
    both = both.astype(BF16)
    mixed_v[...] = both

    def spread(part):
        for k in range(PAIRS // 2):
            src = iota((ROWS, 256), 0)
            dst = iota((ROWS, 256), 1) + 256 * k
            pick = ((src % GROUPS == dst // ENTRIES) & (src < 2 * GROUPS)).astype(F32).astype(BF16)
            wide = jnp.dot(
                mixed_v[ROWS * part : ROWS * (part + 1), :], pick, preferred_element_type=F32
            )
            expf_v[part, 2 * k] = wide[:, :ROWS]
            expf_v[part, 2 * k + 1] = wide[:, ROWS:]

    spread(0)

    ph = unit
    for b in range(8):
        bt_v[0, pl.ds(b, PAIRS, 8), :] = ph[0]
        bt_v[1, pl.ds(b, PAIRS, 8), :] = ph[1]
        mag = jnp.exp(-rate * float(b + 1))
        bt_v[2, pl.ds(b, PAIRS, 8), :] = mag
        bt_v[3, pl.ds(b, PAIRS, 8), :] = 1.0 / mag
        ph8 = ph
        ph = cmul(ph, unit)
    ph = (jnp.ones_like(cos1), jnp.zeros_like(cos1))
    for a in range(8, 16):
        at_v[0, a], at_v[1, a] = ph
        mag = jnp.exp(-rate * float(8 * (a - 8)))
        at_v[2, a], at_v[3, a] = mag, 1.0 / mag
        ph = cmul(ph, ph8)
        back = 16 - (a + 1)
        at_v[0, back], at_v[1, back] = ph[0], -ph[1]
        mag = jnp.exp(rate * float(8 * (8 - back)))
        at_v[2, back], at_v[3, back] = mag, 1.0 / mag

    def table(part, store):
        @pl.loop(0, PAIRS)
        def _(r):
            cb, sb, mb = (bt_v[k, pl.ds(r * 8, 8), :] for k in (0, 1, 3 - part))
            for a in range(16):
                ca, sa, ma = (
                    jnp.broadcast_to(at_v[k, a, pl.ds(r, 1), :], (8, ROWS)) for k in (0, 1, 3 - part)
                )
                c, s = cmul((ca, sa), (cb, sb))
                span = slice(8 * a, 8 * a + 8)
                store(r, span, c, s, ma * mb * expf_v[part, r, span, :])

    def backward(r, span, c, s, scale):
        wneg_v[0, r, span, :] = c * scale
        wneg_v[1, r, span, :] = -s * scale

    def forward(r, span, c, s, scale):
        wpos_v[0, r, span, :] = c * scale
        wpos_v[1, r, span, :] = s * scale

    table(0, backward)
    mid_wide, rest_wide = expand([mid, sigma - mid])
    p64 = power(64)
    end = cmul((at_v[0, 15], at_v[1, 15]), ph8)
    fall = jnp.exp(rest_wide) * jnp.exp(-rate * 64.0)
    last = (end[0] * fall, end[1] * fall)
    enter = (p64[0] * jnp.exp(mid_wide), p64[1] * jnp.exp(mid_wide))

    loads[7].wait()
    dec = expm1(-rate) * cos1 - 2.0 * jnp.sin(0.5 * theta) ** 2
    ims = jnp.exp(-rate) * sin1
    den = rate * rate + theta * theta
    zr = (ims * theta - dec * rate) / den
    zi = -(ims * rate + dec * theta) / den
    sum_v[0], sum_v[1] = zr, zi
    mask = iota((32, ROWS), 0) // 16 == iota((32, ROWS), 1) // ENTRIES
    for r in range(PAIRS):
        span = slice(32 * r, 32 * r + 32)
        br, bi = b_v[0, span, :], b_v[1, span, :]
        br = jnp.concatenate([br, br], axis=1)
        bi = jnp.concatenate([bi, bi], axis=1)
        wr, wi = cmul((sum_v[0, r : r + 1, :], sum_v[1, r : r + 1, :]), (br, bi))
        at = 32 * (r % 4)
        for k, w in enumerate((wr, wi)):
            lanes = slice(ROWS * k, ROWS * (k + 1))
            high, low = split(jnp.where(mask, w, 0.0))
            bw_v[r // 4, at : at + 32, lanes] = high
            bw_v[r // 4, ROWS + at : ROWS + at + 32, lanes] = low

    own_scaled, own_sq = half(tp)
    loads[2].wait()
    acc_v[...] = jnp.dot(
        own_scaled, win_v[pl.ds(tp * HALF, HALF), :], preferred_element_type=F32
    )

    if around:
        pl.semaphore_wait(ring2, len(around))
    sx[0]()
    for dev in far:
        pl.semaphore_signal(ring3, inc=1, device_id=dev)
    if nz > 2:
        pl.semaphore_wait(zring2, beside(1))
        tell(zring3, 2)

    tok_copy.wait_recv()
    gain_copy.wait_recv()
    far_scaled, far_sq = half(other)
    inv = lax.rsqrt((own_sq + far_sq) / D + 1e-06)
    loads[6].wait()
    acc = acc_v[...] + jnp.dot(
        far_scaled, win_v[pl.ds(other * HALF, HALF), :], preferred_element_type=F32
    )
    u_v[...] = (acc * inv).astype(BF16)

    quarter = iota((ROWS, ROWS), 1) // 32
    for j in range(4):
        uj = u_v[:, ROWS * j : ROWS * (j + 1)]
        stacked = jnp.concatenate(
            [jnp.where(quarter == i, uj, jnp.zeros_like(uj)) for i in range(4)], axis=0
        )
        drive = jnp.dot(
            jnp.concatenate([stacked, stacked], axis=1), bw_v[j], preferred_element_type=F32
        )
        for i in range(4):
            r = 4 * j + i
            d = drive[ROWS * i : ROWS * (i + 1)]
            q = cmul((wneg_v[0, r], wneg_v[1, r]), (d[:, :ROWS], d[:, ROWS:]))
            sum_v[0, r : r + 1, :] = jnp.sum(q[0], axis=0, keepdims=True)
            sum_v[1, r : r + 1, :] = jnp.sum(q[1], axis=0, keepdims=True)
            q_v[r, :, 0:ROWS] = q[0]
            q_v[r, :, ROWS:] = q[1]
    mine = cmul(last, (sum_v[0], sum_v[1]))

    def put(buf, index, value):
        buf[index, 0:PAIRS, :] = value[0]
        buf[index, PAIRS : 2 * PAIRS, :] = value[1]

    def take(buf, index):
        return (buf[index, 0:PAIRS, :], buf[index, PAIRS : 2 * PAIRS, :])

    put(mx_v, x, mine)
    mx[0]()

    sx[1]()
    rows = [sx_v[k] for k in range(nx)]
    rho = functools.reduce(jnp.add, rows)
    sy_v[y] = rho
    if far:
        pl.semaphore_wait(ring3, len(far))
    sy[0]()
    wide = expand(rows)
    p128 = power(ROWS)
    ax = [(p128[0] * jnp.exp(w), p128[1] * jnp.exp(w)) for w in wide]

    def sweep(steps, values, start, here):
        total = before = start
        for k in range(len(steps)):
            if k:
                before = tuple(jnp.where(here == k, t, b) for t, b in zip(total, before))
            total = cmul(steps[k], total)
            if values is not None:
                total = cadd(total, values[k])
        return before, total

    one = (jnp.ones_like(cos1), jnp.zeros_like(cos1))
    zero = (jnp.zeros_like(cos1), jnp.zeros_like(cos1))
    dx, _ = sweep(ax, None, one, x)

    def project(w):
        acc = jnp.dot(own_scaled, w[pl.ds(tp * HALF, HALF), :], preferred_element_type=F32)
        acc = acc + jnp.dot(far_scaled, w[pl.ds(other * HALF, HALF), :], preferred_element_type=F32)
        return (acc * inv).astype(BF16).astype(F32)

    loads[8].wait()
    loads[9].wait()
    pad_v[8:, :] = project(wc_v) * project(wv_v)
    index = (z * ny + y) * nx + x
    count = nz * ny * nx
    x1 = lax.rem(x + 1, nx)
    carry = x + 1 == nx
    y1 = jnp.where(carry, lax.rem(y + 1, ny), y)
    z1 = jnp.where(carry & (y + 1 == ny), lax.rem(z + 1, nz), z)
    tail_copy = pltpu.make_async_remote_copy(
        pad_v.at[ROWS : ROWS + 8],
        pad_v.at[0:8],
        tail_sem.at[0],
        tail_sem.at[1],
        device_id={"sz": z1, "sy": y1, "sx": x1},
    )
    pl.when(index + 1 < count)(tail_copy.start)

    spread(1)
    table(1, forward)
    if nz > 2:

        @pl.when(beside(2) > 0)
        def _():
            pl.semaphore_wait(zring3, beside(2))

    if nz > 4:
        tell(zring4, 4, above=False)

    mx[1]()
    pre_x, row_total = sweep(ax, [take(mx_v, k) for k in range(nx)], zero, x)
    put(my_v, y, row_total)
    my[0]()

    sy[1]()
    rows = [sy_v[k] for k in range(ny)]
    pi = functools.reduce(jnp.add, rows)
    sz_v[z] = pi
    if nz > 4:

        @pl.when(z + 4 < nz)
        def _():
            pl.semaphore_wait(zring4, 1)

    sz[0]()
    p512 = power(ROWS * nx)
    ay = [(p512[0] * jnp.exp(w), p512[1] * jnp.exp(w)) for w in expand(rows)]
    dy, _ = sweep(ay, None, one, y)
    pz = power(ROWS * nx * ny)

    loads[10].wait()
    for r in range(PAIRS):
        span = slice(32 * r, 32 * r + 32)
        cr, ci = c_v[0, span, :], c_v[1, span, :]
        cw_v[span, 0:ROWS] = jnp.where(mask, jnp.concatenate([cr, cr], axis=1), 0.0)
        cw_v[span, ROWS:] = jnp.where(mask, jnp.concatenate([ci, ci], axis=1), 0.0)
    tri16 = jnp.concatenate([tri.astype(BF16), tri.astype(BF16)], axis=1)
    sign = jnp.where(iota((1, 256), 1) < ROWS, 1.0, -1.0)
    nt = (((1,), (1,)), ((), ()))

    def gathered(wide):
        total = jnp.where(quarter == 0, wide[0:ROWS], 0.0)
        for i in range(1, 4):
            total = jnp.where(quarter == i, wide[ROWS * i : ROWS * (i + 1)], total)
        return total

    def read_out(high, low, weights):
        wide = lax.dot_general(high, weights, nt, preferred_element_type=F32)
        rest = lax.dot_general(low, weights[0:ROWS], nt, preferred_element_type=F32)
        return gathered(wide[:, :ROWS] + wide[:, ROWS:] + rest)

    loads[13].wait()
    for j in range(4):
        highs, lows = [], []
        for i in range(4):
            r = 4 * j + i
            pre = jnp.dot(
                tri16, jnp.concatenate(split(q_v[r]), axis=0), preferred_element_type=F32
            )
            st = cmul((wpos_v[0, r], wpos_v[1, r]), (pre[:, :ROWS], pre[:, ROWS:]))
            high, low = zip(*(split(part) for part in st))
            highs.append(jnp.concatenate(high, axis=1))
            lows.append(jnp.concatenate(low, axis=1))
            for k in range(2):
                lanes = slice(ROWS * k, ROWS * (k + 1))
                span = slice(ROWS * r, ROWS * (r + 1))
                wposb_v[0, span, lanes], wposb_v[1, span, lanes] = split(wpos_v[k, r])
        cols = slice(ROWS * j, ROWS * (j + 1))
        weights = jnp.concatenate(split(cw_v[cols, :] * sign), axis=0)
        read = read_out(jnp.concatenate(highs, axis=0), jnp.concatenate(lows, axis=0), weights)
        ypre_v[:, cols] = read + skip_v[:, cols] * u_v[:, cols].astype(F32)

    my[1]()
    pre_y, plane_total = sweep(ay, [take(my_v, k) for k in range(ny)], zero, y)
    put(mz_v, z, plane_total)
    mz[0]()

    loads[11].wait()
    bg_v[...] = project(wb_v)

    @pl.when(index == 0)
    def _():
        pad_v[0:8, :] = jnp.zeros((8, CH), F32)

    pl.when(index > 0)(tail_copy.wait_recv)
    loads[15].wait()
    loads[16].wait()
    conv = pad_v[6 : 6 + ROWS, :] * taps_v[0:1, :]
    conv = conv + pad_v[7 : 7 + ROWS, :] * taps_v[1:2, :]
    conv = conv + pad_v[8 : 8 + ROWS, :] * taps_v[2:3, :]

    def head_norm(values, gain, width):
        same = iota((ROWS, ROWS), 0) // width == iota((ROWS, ROWS), 1) // width
        mean = jnp.where(same, 1.0 / width, 0.0).astype(BF16)
        mean = jnp.concatenate([mean, mean], axis=0)
        pieces = []
        for j in range(4):
            cols = slice(ROWS * j, ROWS * (j + 1))
            v = values[:, cols]
            m = jnp.dot(
                jnp.concatenate(split(v * v), axis=1), mean, preferred_element_type=F32
            )
            pieces.append((v * lax.rsqrt(m + 1e-06) * gain[:, cols]).astype(BF16))
        return jnp.concatenate(pieces, axis=1)

    conv_out = head_norm(bg_v[...] * conv, cgain_v[...], 64)
    loads[17].wait()
    for c in range(4):
        cpart_v[:, CH * c : CH * (c + 1)] = jnp.dot(
            conv_out, woc_v[:, CH * c : CH * (c + 1)], preferred_element_type=F32
        )

    sz[1]()
    az = [(pz[0] * jnp.exp(w), pz[1] * jnp.exp(w)) for w in expand([sz_v[k] for k in range(nz)])]
    loads[12].wait()
    start = (paired(init_v, (0,)), paired(init_v, (1,)))
    loads[14].wait()
    loads[18].wait()

    mz[1]()
    pre_z, _ = sweep(az, [take(mz_v, k) for k in range(nz)], start, z)
    entry = cadd(cmul(dx, cadd(cmul(dy, pre_z), pre_y)), pre_x)
    entry = cmul(enter, entry)
    sum_v[0], sum_v[1] = entry
    for r in range(PAIRS):
        span = slice(32 * r, 32 * r + 32)
        ce = cmul(
            (sum_v[0, r : r + 1, :], sum_v[1, r : r + 1, :]), (cw_v[span, 0:ROWS], cw_v[span, ROWS:])
        )
        at = 32 * (r % 4)
        for k, w in enumerate((ce[0], -ce[1])):
            lanes = slice(ROWS * k, ROWS * (k + 1))
            high, low = split(w)
            ce_v[r // 4, at : at + 32, lanes] = high
            ce_v[r // 4, ROWS + at : ROWS + at + 32, lanes] = low
    acts = []
    for j in range(4):
        cols = slice(ROWS * j, ROWS * (j + 1))
        span = slice(4 * ROWS * j, 4 * ROWS * (j + 1))
        pre = ypre_v[:, cols] + read_out(wposb_v[0, span, :], wposb_v[1, span, :], ce_v[j])
        acts.append(0.5 * pre * (1.0 + lax.erf(pre * math.sqrt(0.5))))
    sout_v[...] = head_norm(jnp.concatenate(acts, axis=1), sgain_v[...], 16)

    sends = []
    for c in range(4):
        cols = slice(CH * c, CH * (c + 1))
        part = jnp.dot(sout_v[...], wos_v[:, cols], preferred_element_type=F32) + cpart_v[:, cols]
        part_v[c] = part.astype(BF16)
        send = pltpu.make_async_remote_copy(
            part_v.at[c, pl.ds(other * 64, 64)],
            got_v.at[c],
            part_ss.at[c],
            part_rs.at[c],
            device_id={"tp": other},
        )
        send.start()
        sends.append(send)
    for c in range(4):
        cols = slice(CH * c, CH * (c + 1))
        sends[c].wait_recv()
        own = part_v[c, pl.ds(tp * 64, 64), :].astype(F32)
        out[:, cols] = (own + got_v[c].astype(F32)).astype(BF16)
    for c in range(4):
        sends[c].wait_send()
    tok_copy.wait_send()
    gain_copy.wait_send()
    pl.when(index + 1 < count)(tail_copy.wait_send)
    for ex in (sx, sy, sz, mx, my, mz):
        ex[2]()


def body(dims, *args):
    args = list(args)
    args[9] = jnp.swapaxes(args[9], 2, 3).reshape(2, CH, ENTRIES)
    args[10] = args[10].reshape(2, CH, ENTRIES)
    for k in (12, 13, 14):
        args[k] = args[k].reshape(1, CH)
    args = [pltpu.with_memory_space_constraint(a, pltpu.MemorySpace.HBM) for a in args]
    nz, ny, nx = dims
    anyspace = pl.BlockSpec(memory_space=pltpu.MemorySpace.HBM)
    vm = pltpu.VMEM
    dma = pltpu.SemaphoreType.DMA
    scratch = [
        vm((2, ROWS, HALF), BF16),
        vm((2, 1, HALF), BF16),
        vm((D, CH), BF16),
        vm((D, CH), BF16),
        vm((D, CH), BF16),
        vm((D, CH), BF16),
        vm((GROUPS, ENTRIES), F32),
        vm((GROUPS, ENTRIES), F32),
        vm((GROUPS, ROWS), F32),
        vm((2, CH, ENTRIES), F32),
        vm((2, CH, ENTRIES), F32),
        vm((2, GROUPS, ENTRIES), F32),
        vm((1, CH), F32),
        vm((1, CH), F32),
        vm((1, CH), F32),
        vm((3, CH), F32),
        vm((CH, D), BF16),
        vm((CH, D), BF16),
        vm((ROWS, CH), F32),
        vm((ROWS, CH), BF16),
        vm((4, 256, 256), BF16),
        vm((CH, 256), F32),
        vm((4, 256, 256), BF16),
        vm((2, PAIRS, ROWS, ROWS), F32),
        vm((4, 16, PAIRS, ROWS), F32),
        vm((4, ROWS, ROWS), F32),
        vm((2, PAIRS, ROWS, ROWS), F32),
        vm((2, PAIRS, ROWS, ROWS), F32),
        vm((2, PAIRS * ROWS, 256), BF16),
        vm((PAIRS, ROWS, 256), F32),
        vm((2, PAIRS, ROWS), F32),
        vm((256, ROWS), BF16),
        vm((ROWS, CH), F32),
        vm((ROWS + 8, CH), F32),
        vm((ROWS, CH), F32),
        vm((ROWS, D), F32),
        vm((ROWS, CH), BF16),
        vm((4, ROWS, CH), BF16),
        vm((4, 64, CH), BF16),
        vm((nx, 1, ROWS), F32),
        vm((ny, 1, ROWS), F32),
        vm((nz, 1, ROWS), F32),
        vm((nx, 32, ROWS), F32),
        vm((ny, 32, ROWS), F32),
        vm((nz, 32, ROWS), F32),
        dma((19,)),
        dma((4,)),
        dma((2,)),
        dma((4,)),
        dma((4,)),
        dma((2, nx)),
        dma((2, ny)),
        dma((2, nz)),
        dma((2, nx)),
        dma((2, ny)),
        dma((2, nz)),
        *[pltpu.SemaphoreType.REGULAR] * 5,
    ]
    return pl.pallas_call(
        functools.partial(kernel, dims),
        out_shape=jax.ShapeDtypeStruct((64, D), BF16),
        in_specs=[anyspace] * len(args),
        out_specs=pl.BlockSpec(memory_space=pltpu.MemorySpace.VMEM),
        scratch_shapes=scratch,
        compiler_params=pltpu.CompilerParams(
            collective_id=0, has_side_effects=True, vmem_limit_bytes=48 * 1024 * 1024
        ),
        name="layer",
    )(*args)


def solution(mesh):
    dims = SP_DIMS
    finer = Mesh(mesh.devices.reshape(*dims, mesh.shape["tp"]), (*SP, "tp"))
    placed = (
        P(SP, "tp"),
        P(None, "tp"),
        P(None, "tp"),
        P(None, "tp"),
        P(None, "tp"),
        P(None, "tp"),
        P("tp", None),
        P("tp", None),
        P("tp", SP),
        P(None, "tp", None, None),
        P(None, "tp", None, None),
        P(None, "tp", None),
        P("tp"),
        P("tp"),
        P("tp"),
        P(None, "tp"),
        P("tp", None),
        P("tp", None),
    )
    return jax.shard_map(
        functools.partial(body, dims),
        mesh=finer,
        in_specs=placed,
        out_specs=P((*SP, "tp"), None),
        check_vma=False,
    )
```

profile of v0, /device:TPU:1, one launch (start us, length us, event | category | flops | bytes accessed | tf_op | source)
XLA Modules:
  0.0 30.7 jit_solution(7611486350357803564)
XLA Ops:
  0.0 30.0 %layer.1 = bf16[64,2048]{1,0:T(8,128)(2,1)S(1)} custom-call(bf16[128,1024]{1,0:T(8,128)(2,1)} %tokens.1, bf16[1,1024]{1,0:T(2,128)(2,1)} %in_gain.1, bf16[2048,512]{1,0:T(8,128)(2,1)} %w_input.1, bf16[2048,512]{1,0:T(8,128)(2,1)} %w_bgate.1, bf16[2048,512]{1,0:T(8,128)(2,1)} %w_cgate.1, bf16[2048,512]{1,0:T(8,128)(2,1)} %w_value.1, f32[32,64]{1,0:T(8,128)} %decay_rate.1, ...), custom_call_target="tpu_custom_call" | custom-call | tf_op jit(solution)/shard_map/layer/pallas_call | solution.py:751
  30.0 0.7 %copy.20 = bf16[64,2048]{1,0:T(8,128)(2,1)} copy(bf16[64,2048]{1,0:T(8,128)(2,1)S(1)} %layer.1) | data formatting | bytes 524288
where the time goes:
time: 30.9 us; the launch traced here: 30.7 us
  Pallas kernels  30 us (97%)
  local copies, waits for them, and re-layouts  0.71 us (2%)
    pallas_call x1, Pallas kernels, body(): pl.pallas_call(functools.partial(kernel, dims), out_shape=jax.ShapeDtypeS...  30 us
    unnamed x1, local copies, waits for them, and re-layouts  0.71 us

commit v1 on v0

--- a/solution.py
+++ b/solution.py
@@ -224,8 +224,10 @@
                 device_id=at_step(axis, step),
             )
 
-        def start():
+        def start(first=1, end=n):
             for s in order:
+                if not first <= s < end:
+                    continue
                 if later:
                     pl.when(here + s < n)(copy(s).start)
                 else:
@@ -457,6 +459,16 @@
     put(mx_v, x, mine)
     mx[0]()
 
+    spread(1)
+    table(1, forward)
+    def project(w):
+        acc = jnp.dot(own_scaled, w[pl.ds(tp * HALF, HALF), :], preferred_element_type=F32)
+        acc = acc + jnp.dot(far_scaled, w[pl.ds(other * HALF, HALF), :], preferred_element_type=F32)
+        return (acc * inv).astype(BF16).astype(F32)
+
+    loads[8].wait()
+    loads[9].wait()
+    pad_v[8:, :] = project(wc_v) * project(wv_v)
     sx[1]()
     rows = [sx_v[k] for k in range(nx)]
     rho = functools.reduce(jnp.add, rows)
@@ -464,32 +476,15 @@
     if far:
         pl.semaphore_wait(ring3, len(far))
     sy[0]()
-    wide = expand(rows)
-    p128 = power(ROWS)
-    ax = [(p128[0] * jnp.exp(w), p128[1] * jnp.exp(w)) for w in wide]
-
-    def sweep(steps, values, start, here):
-        total = before = start
-        for k in range(len(steps)):
-            if k:
-                before = tuple(jnp.where(here == k, t, b) for t, b in zip(total, before))
-            total = cmul(steps[k], total)
-            if values is not None:
-                total = cadd(total, values[k])
-        return before, total
-
-    one = (jnp.ones_like(cos1), jnp.zeros_like(cos1))
-    zero = (jnp.zeros_like(cos1), jnp.zeros_like(cos1))
-    dx, _ = sweep(ax, None, one, x)
-
-    def project(w):
-        acc = jnp.dot(own_scaled, w[pl.ds(tp * HALF, HALF), :], preferred_element_type=F32)
-        acc = acc + jnp.dot(far_scaled, w[pl.ds(other * HALF, HALF), :], preferred_element_type=F32)
-        return (acc * inv).astype(BF16).astype(F32)
-
-    loads[8].wait()
-    loads[9].wait()
-    pad_v[8:, :] = project(wc_v) * project(wv_v)
+    if nz > 2:
+
+        @pl.when(beside(2) > 0)
+        def _():
+            pl.semaphore_wait(zring3, beside(2))
+
+    if nz > 4:
+        tell(zring4, 4, above=False)
+
     index = (z * ny + y) * nx + x
     count = nz * ny * nx
     x1 = lax.rem(x + 1, nx)
@@ -505,37 +500,28 @@
     )
     pl.when(index + 1 < count)(tail_copy.start)
 
-    spread(1)
-    table(1, forward)
-    if nz > 2:
-
-        @pl.when(beside(2) > 0)
-        def _():
-            pl.semaphore_wait(zring3, beside(2))
-
-    if nz > 4:
-        tell(zring4, 4, above=False)
+    wide = expand(rows)
+    p128 = power(ROWS)
+    ax = [(p128[0] * jnp.exp(w), p128[1] * jnp.exp(w)) for w in wide]
+
+    def sweep(steps, values, start, here):
+        total = before = start
+        for k in range(len(steps)):
+            if k:
+                before = tuple(jnp.where(here == k, t, b) for t, b in zip(total, before))
+            total = cmul(steps[k], total)
+            if values is not None:
+                total = cadd(total, values[k])
+        return before, total
+
+    one = (jnp.ones_like(cos1), jnp.zeros_like(cos1))
+    zero = (jnp.zeros_like(cos1), jnp.zeros_like(cos1))
+    dx, _ = sweep(ax, None, one, x)
 
     mx[1]()
     pre_x, row_total = sweep(ax, [take(mx_v, k) for k in range(nx)], zero, x)
     put(my_v, y, row_total)
     my[0]()
-
-    sy[1]()
-    rows = [sy_v[k] for k in range(ny)]
-    pi = functools.reduce(jnp.add, rows)
-    sz_v[z] = pi
-    if nz > 4:
-
-        @pl.when(z + 4 < nz)
-        def _():
-            pl.semaphore_wait(zring4, 1)
-
-    sz[0]()
-    p512 = power(ROWS * nx)
-    ay = [(p512[0] * jnp.exp(w), p512[1] * jnp.exp(w)) for w in expand(rows)]
-    dy, _ = sweep(ay, None, one, y)
-    pz = power(ROWS * nx * ny)
 
     loads[10].wait()
     for r in range(PAIRS):
@@ -579,11 +565,6 @@
         read = read_out(jnp.concatenate(highs, axis=0), jnp.concatenate(lows, axis=0), weights)
         ypre_v[:, cols] = read + skip_v[:, cols] * u_v[:, cols].astype(F32)
 
-    my[1]()
-    pre_y, plane_total = sweep(ay, [take(my_v, k) for k in range(ny)], zero, y)
-    put(mz_v, z, plane_total)
-    mz[0]()
-
     loads[11].wait()
     bg_v[...] = project(wb_v)
 
@@ -619,12 +600,41 @@
             conv_out, woc_v[:, CH * c : CH * (c + 1)], preferred_element_type=F32
         )
 
+    sy[1]()
+    rows = [sy_v[k] for k in range(ny)]
+    pi = functools.reduce(jnp.add, rows)
+    sz_v[z] = pi
+    sz[0](1, 5)
+    p512 = power(ROWS * nx)
+    ay = [(p512[0] * jnp.exp(w), p512[1] * jnp.exp(w)) for w in expand(rows)]
+    dy, _ = sweep(ay, None, one, y)
+    pz = power(ROWS * nx * ny)
+
+    my[1]()
+    pre_y, plane_total = sweep(ay, [take(my_v, k) for k in range(ny)], zero, y)
+    put(mz_v, z, plane_total)
+    mz[0](1, 5)
+    if nz > 4:
+
+        @pl.when(z + 4 < nz)
+        def _():
+            pl.semaphore_wait(zring4, 1)
+
+        sz[0](5, nz)
+        mz[0](5, nz)
+
     sz[1]()
     az = [(pz[0] * jnp.exp(w), pz[1] * jnp.exp(w)) for w in expand([sz_v[k] for k in range(nz)])]
     loads[12].wait()
     start = (paired(init_v, (0,)), paired(init_v, (1,)))
     loads[14].wait()
     loads[18].wait()
+
+    tok_copy.wait_send()
+    gain_copy.wait_send()
+    pl.when(index + 1 < count)(tail_copy.wait_send)
+    for ex in (sx, mx, sy, my):
+        ex[2]()
 
     mz[1]()
     pre_z, _ = sweep(az, [take(mz_v, k) for k in range(nz)], start, z)
@@ -664,6 +674,8 @@
         )
         send.start()
         sends.append(send)
+    sz[2]()
+    mz[2]()
     for c in range(4):
         cols = slice(CH * c, CH * (c + 1))
         sends[c].wait_recv()
@@ -671,11 +683,6 @@
         out[:, cols] = (own + got_v[c].astype(F32)).astype(BF16)
     for c in range(4):
         sends[c].wait_send()
-    tok_copy.wait_send()
-    gain_copy.wait_send()
-    pl.when(index + 1 < count)(tail_copy.wait_send)
-    for ex in (sx, sy, sz, mx, my, mz):
-        ex[2]()
 
 
 def body(dims, *args):

time: 30.9 us -> 27.7 us (0.90)
  the two profiles are of different devices: /device:TPU:1 before, /device:TPU:193 now
where the time goes in v1:
time: 27.7 us; the launch traced here: 27.6 us
  Pallas kernels  26.9 us (97%)
  local copies, waits for them, and re-layouts  0.71 us (3%)
    pallas_call x1, Pallas kernels, body(): pl.pallas_call(functools.partial(kernel, dims), out_shape=jax.ShapeDtypeS...  26.9 us
    unnamed x1, local copies, waits for them, and re-layouts  0.71 us

profile of v1, /device:TPU:193, one launch (start us, length us, event | category | flops | bytes accessed | tf_op | source)
XLA Modules:
  0.0 27.6 jit_solution(11102277629777714459)
XLA Ops:
  0.0 26.9 %layer.1 = bf16[64,2048]{1,0:T(8,128)(2,1)S(1)} custom-call(bf16[128,1024]{1,0:T(8,128)(2,1)} %tokens.1, bf16[1,1024]{1,0:T(2,128)(2,1)} %in_gain.1, bf16[2048,512]{1,0:T(8,128)(2,1)} %w_input.1, bf16[2048,512]{1,0:T(8,128)(2,1)} %w_bgate.1, bf16[2048,512]{1,0:T(8,128)(2,1)} %w_cgate.1, bf16[2048,512]{1,0:T(8,128)(2,1)} %w_value.1, f32[32,64]{1,0:T(8,128)} %decay_rate.1, ...), custom_call_target="tpu_custom_call" | custom-call | tf_op jit(solution)/shard_map/layer/pallas_call | solution.py:758
  26.9 0.7 %copy.20 = bf16[64,2048]{1,0:T(8,128)(2,1)} copy(bf16[64,2048]{1,0:T(8,128)(2,1)S(1)} %layer.1) | data formatting | bytes 524288

commit v2 on v1

--- a/solution.py
+++ b/solution.py
@@ -173,16 +173,14 @@
     far = [at_step("sx", s) for s in near("sx")]
     far += [at_step("sy", s) for s in (2, 6) if ny == 8]
 
-    def tell(sem, step, above=True):
+    def tell(sem, step):
         @pl.when(z >= step)
         def _():
             pl.semaphore_signal(sem, inc=1, device_id={"sz": z - step})
 
-        if above:
-
-            @pl.when(z + step < nz)
-            def _():
-                pl.semaphore_signal(sem, inc=1, device_id={"sz": z + step})
+        @pl.when(z + step < nz)
+        def _():
+            pl.semaphore_signal(sem, inc=1, device_id={"sz": z + step})
 
     def beside(step):
         return jnp.where(z + step < nz, 1, 0) + jnp.where(z >= step, 1, 0)
@@ -469,6 +467,19 @@
     loads[8].wait()
     loads[9].wait()
     pad_v[8:, :] = project(wc_v) * project(wv_v)
+    if nz > 2:
+
+        @pl.when(beside(2) > 0)
+        def _():
+            pl.semaphore_wait(zring3, beside(2))
+
+    if nz > 4:
+
+        @pl.when((z >= 4) & (z + 1 < nz))
+        def _():
+            pl.semaphore_signal(zring4, inc=1, device_id={"sz": z - 4})
+
+
     sx[1]()
     rows = [sx_v[k] for k in range(nx)]
     rho = functools.reduce(jnp.add, rows)
@@ -476,15 +487,6 @@
     if far:
         pl.semaphore_wait(ring3, len(far))
     sy[0]()
-    if nz > 2:
-
-        @pl.when(beside(2) > 0)
-        def _():
-            pl.semaphore_wait(zring3, beside(2))
-
-    if nz > 4:
-        tell(zring4, 4, above=False)
-
     index = (z * ny + y) * nx + x
     count = nz * ny * nx
     x1 = lax.rem(x + 1, nx)
@@ -616,7 +618,7 @@
     mz[0](1, 5)
     if nz > 4:
 
-        @pl.when(z + 4 < nz)
+        @pl.when(z + 5 < nz)
         def _():
             pl.semaphore_wait(zring4, 1)
 

time: 27.7 us -> 27.7 us (level)
  no operation moved by 1% of the time
where the time goes in v2:
time: 27.7 us; the launch traced here: 27.6 us
  Pallas kernels  26.9 us (97%)
  local copies, waits for them, and re-layouts  0.71 us (3%)
    pallas_call x1, Pallas kernels, body(): pl.pallas_call(functools.partial(kernel, dims), out_shape=jax.ShapeDtypeS...  26.9 us
    unnamed x1, local copies, waits for them, and re-layouts  0.71 us

profile of v2, /device:TPU:193, one launch (start us, length us, event | category | flops | bytes accessed | tf_op | source)
XLA Modules:
  0.0 27.6 jit_solution(6591648038722190885)
XLA Ops:
  0.0 26.9 %layer.1 = bf16[64,2048]{1,0:T(8,128)(2,1)S(1)} custom-call(bf16[128,1024]{1,0:T(8,128)(2,1)} %tokens.1, bf16[1,1024]{1,0:T(2,128)(2,1)} %in_gain.1, bf16[2048,512]{1,0:T(8,128)(2,1)} %w_input.1, bf16[2048,512]{1,0:T(8,128)(2,1)} %w_bgate.1, bf16[2048,512]{1,0:T(8,128)(2,1)} %w_cgate.1, bf16[2048,512]{1,0:T(8,128)(2,1)} %w_value.1, f32[32,64]{1,0:T(8,128)} %decay_rate.1, ...), custom_call_target="tpu_custom_call" | custom-call | tf_op jit(solution)/shard_map/layer/pallas_call | solution.py:760
  26.9 0.7 %copy.20 = bf16[64,2048]{1,0:T(8,128)(2,1)} copy(bf16[64,2048]{1,0:T(8,128)(2,1)S(1)} %layer.1) | data formatting | bytes 524288
